TPU v7x, 512 devices: a whole 4x4x16 slice. The times are simulated.
512 devices in a mesh: ep: 32 (over z, core), tp: 16 (over y, x).
Axes of the slice: x: 4, y: 4, z: 16, core: 2. Of those that a mesh axis runs over, the one named last changes fastest.
Arguments:
- queries: bfloat16 [8192, 2048], P('ep', 'tp'), may hold values from -6 to 6
- key_rows: bfloat16 [8192, 1024], P('ep', 'tp'), may hold values from -6 to 6
- values: bfloat16 [8192, 1024], P('ep', 'tp'), may hold values from -140 to 140
- query_gain: float32 [64], replicated, may hold values from 0.55 to 7.5
- key_gain: float32 [64], replicated, may hold values from 0.55 to 7.5
- mix_gain: float32 [2048], replicated, may hold values from 0.1 to 1.9
- out_weight: bfloat16 [2048, 4096], P(None, 'tp'), may hold values from -0.125 to 0.125
- expert_input: bfloat16 [8192, 4096], P('ep', 'tp'), may hold values from -140 to 140
- expert_gain: float32 [4096], replicated, may hold values from 0.1 to 1.9
- route_ids: int32 [8192, 2], P('ep'), may hold values from 0 to 31, as said below
- route_weights: float32 [8192, 2], P('ep'), may hold values from 0.3 to 1.7
- expert_gate: bfloat16 [32, 4096, 2048], P('ep', None, 'tp'), may hold values from -0.09375 to 0.09375
- expert_up: bfloat16 [32, 4096, 2048], P('ep', None, 'tp'), may hold values from -0.09375 to 0.09375
- expert_down: bfloat16 [32, 2048, 4096], P('ep', None, 'tp'), may hold values from -0.125 to 0.125
Outputs:
- attended: bfloat16 [8192, 4096], P('ep', 'tp')
- expert_mix: bfloat16 [8192, 4096], P('ep', 'tp')
Inputs may be any that keep to these rules, and one draw needn't show every extreme that they name: `route_ids`: the 2 experts of a row differ. In every aligned block of 256 rows no expert is named more than 22 times, and one expert, the same for all blocks, is named exactly 22 times in every block.
All inputs are finite; a program needn't handle non-finite values.
Results may differ from a plain program's by a relative error of at most 0.01.
The roundings to bfloat16 on the way count: a program that leaves them out, or rounds other values in their place, can miss the bound.
Values may be sent and summed in bfloat16 or wider, within the bound.
A program may use at most 64 MiB of HBM per device.

v0:
```python
import math
import jax
import jax.numpy as jnp
from jax import lax
from jax.sharding import Mesh
from jax.sharding import PartitionSpec as P

Q_HEADS = 32
KV_HEADS = 16
HEAD = 64
GRID_W = 64
EP = ("ep_0", "ep_1")
EPS = 1e-06
THETA = 10000.0


def in_one_piece(arrays, axis, dim, along):
    widths = [a.shape[along] for a in arrays]
    both = jnp.concatenate(arrays, axis=along)
    filled = lax.all_gather(both, axis, axis=dim, tiled=True)
    return tuple(jnp.split(filled, [sum(widths[:k]) for k in range(1, len(widths))], axis=along))


def split_up(array, dim, length):
    before, after = (array.shape[:dim], array.shape[dim + 1 :])
    return jnp.moveaxis(array.reshape(*before, length, -1, *after), dim, 0)


def joined_along(blocks, dim):
    lengths = list(blocks.shape[1:])
    lengths[dim] *= blocks.shape[0]
    return jnp.moveaxis(blocks, 0, dim).reshape(lengths)


def exchange_in_order(blocks, axes, order):
    inside = blocks.shape[1:]
    filled = blocks.reshape(*(lax.axis_size(a) for a in axes), *inside)
    for k in order:
        filled = lax.all_to_all(filled, axes[k], k, k, tiled=True)
    return filled.reshape(-1, *inside)


def exchange_by_chip(array, groups, order, split_dim, concat_dim):
    length = lax.axis_size(groups[0]) * lax.axis_size(groups[1])
    blocks = split_up(array, split_dim, length)
    return joined_along(exchange_in_order(blocks, groups, order), concat_dim)


def turn_tables(offset, length):
    half_width = HEAD // 2
    inverse = THETA ** (-jnp.arange(0, half_width, 2, dtype=jnp.float32) / half_width)
    positions = offset + jnp.arange(length, dtype=jnp.int32)
    grid_rows = (positions // GRID_W).astype(jnp.float32)
    grid_cols = (positions % GRID_W).astype(jnp.float32)
    angles = jnp.concatenate([grid_rows[:, None] * inverse, grid_cols[:, None] * inverse], axis=-1)
    return (jnp.cos(angles), jnp.sin(angles))


def norm_turn(source, scale_gain, cosine_table, sine_table):
    length = source.shape[0]
    head_rows = source.astype(jnp.float32).reshape(length, -1, HEAD)
    head_rows = (
        head_rows
        * lax.rsqrt(jnp.mean(head_rows * head_rows, axis=-1, keepdims=True) + EPS)
        * scale_gain
    )
    pair_view = head_rows.reshape(length, head_rows.shape[1], HEAD // 2, 2)
    even_part = pair_view[..., 0]
    odd_part = pair_view[..., 1]
    cosine_part = cosine_table[:, None, :]
    sine_part = sine_table[:, None, :]
    turned = jnp.stack(
        [
            even_part * cosine_part - odd_part * sine_part,
            even_part * sine_part + odd_part * cosine_part,
        ],
        axis=-1,
    )
    return turned.reshape(length, -1).astype(jnp.bfloat16)


def shards(
    queries,
    key_rows,
    values,
    query_gain,
    key_gain,
    mix_gain,
    out_weight,
    expert_input,
    expert_gain,
    route_ids,
    route_weights,
    expert_gate,
    expert_up,
    expert_down,
):
    length = queries.shape[0]
    experts_count = lax.axis_size(EP)
    offset = lax.axis_index(EP) * length
    cosine_table, sine_table = turn_tables(offset, length)
    query_turned = norm_turn(queries, query_gain, cosine_table, sine_table)
    key_turned = norm_turn(key_rows, key_gain, cosine_table, sine_table)
    kv_local = key_rows.shape[1] // HEAD
    group_size = Q_HEADS // KV_HEADS
    query_heads = query_turned.reshape(length, kv_local, group_size, HEAD)
    start_state = (
        jnp.full((kv_local, group_size, length), -jnp.inf, jnp.float32),
        jnp.zeros((kv_local, group_size, length), jnp.float32),
        jnp.zeros((length, kv_local, group_size, HEAD), jnp.float32),
    )
    key_piece, value_piece = in_one_piece((key_turned, values), EP, 0, 1)
    piece_rows = key_piece.shape[0]
    step_rows = 1024
    key_blocks = key_piece.reshape(piece_rows // step_rows, step_rows, kv_local, HEAD)
    value_blocks = value_piece.reshape(piece_rows // step_rows, step_rows, kv_local, HEAD)

    def absorb(current, block_pair):
        running_max, running_sum, running_acc = current
        key_block, value_block = block_pair
        scores = jnp.einsum(
            "rhgd,nhd->hgrn", query_heads, key_block, preferred_element_type=jnp.float32
        ) / math.sqrt(HEAD)
        new_max = jnp.maximum(running_max, jnp.max(scores, axis=-1))
        factor = jnp.exp(running_max - new_max)
        raw_weights = jnp.exp(scores - new_max[..., None])
        new_sum = running_sum * factor + jnp.sum(raw_weights, axis=-1)
        rounded = raw_weights.astype(jnp.bfloat16)
        increment = jnp.einsum(
            "hgrn,nhd->rhgd", rounded, value_block, preferred_element_type=jnp.float32
        )
        new_acc = running_acc * jnp.transpose(factor, (2, 0, 1))[..., None] + increment
        return ((new_max, new_sum, new_acc), None)

    result, unused = lax.scan(absorb, start_state, (key_blocks, value_blocks))
    heads_out = (
        (result[2] / jnp.transpose(result[1], (2, 0, 1))[..., None])
        .reshape(length, -1)
        .astype(jnp.bfloat16)
    )
    top_count = route_ids.shape[1]
    copies = route_ids.shape[0] * top_count
    capacity = (4 * copies + 3 * experts_count - 1) // (3 * experts_count)
    slot_total = experts_count * capacity
    flat_ids = route_ids.reshape(copies)
    hit_marks = (flat_ids[:, None] == jnp.arange(experts_count, dtype=jnp.int32)[None, :]).astype(
        jnp.int32
    )
    earlier = jnp.cumsum(hit_marks, axis=0) - hit_marks
    places = jnp.sum(earlier * hit_marks, axis=1)
    slot_index = flat_ids * capacity + places
    slot_rows = (
        jnp.full((slot_total,), route_ids.shape[0], jnp.int32)
        .at[slot_index]
        .set(jnp.arange(copies, dtype=jnp.int32) // top_count)
    )
    width_local = expert_input.shape[1]
    padded = jnp.concatenate([expert_input, jnp.zeros((1, width_local), jnp.bfloat16)], axis=0)
    outgoing = padded[slot_rows].reshape(experts_count, capacity, width_local)
    arrived = exchange_by_chip(outgoing, ("ep_0", "ep_1"), (1, 0), 0, 0).reshape(
        slot_total, width_local
    )
    piece_float = lax.all_gather(arrived, "tp", axis=1, tiled=True).astype(jnp.float32)
    gain_piece = expert_gain
    scaled_piece = (piece_float * gain_piece).astype(jnp.bfloat16)
    gate_rows = expert_gate[0]
    up_rows = expert_up[0]
    gate_sum = jnp.dot(scaled_piece, gate_rows, preferred_element_type=jnp.float32)
    up_sum = jnp.dot(scaled_piece, up_rows, preferred_element_type=jnp.float32)
    square_sum = jnp.sum(piece_float * piece_float, axis=1)
    row_stat = lax.rsqrt(square_sum / expert_gain.shape[0] + EPS)
    gate_value = gate_sum * row_stat[:, None]
    up_value = up_sum * row_stat[:, None]
    hidden = (jax.nn.silu(gate_value) * up_value).astype(jnp.bfloat16)
    width_out = out_weight.shape[1]
    head_piece, hidden_piece = in_one_piece((heads_out, hidden), "tp", 1, 0)
    head_float = head_piece.astype(jnp.float32)
    gain_piece = mix_gain
    mix_in = (head_float * gain_piece).astype(jnp.bfloat16)
    down_rows = expert_down[0]
    mix_sum = jnp.dot(mix_in, out_weight, preferred_element_type=jnp.float32)
    mix_squares = jnp.sum(head_float * head_float, axis=1)
    expert_sum = jnp.dot(hidden_piece, down_rows, preferred_element_type=jnp.float32)
    attended = (mix_sum * lax.rsqrt(mix_squares / mix_gain.shape[0] + EPS)[:, None]).astype(
        jnp.bfloat16
    )
    expert_back = expert_sum.astype(jnp.bfloat16).reshape(experts_count, capacity, width_out)
    returned = lax.all_to_all(expert_back, EP, split_axis=0, concat_axis=0, tiled=True).reshape(
        slot_total, width_out
    )
    picked = returned[slot_index].astype(jnp.float32) * route_weights.reshape(copies)[:, None]
    expert_mix = jnp.sum(picked.reshape(route_ids.shape[0], top_count, width_out), axis=1).astype(
        jnp.bfloat16
    )
    return (attended, expert_mix)


def solution(mesh):
    torus = Mesh(mesh.devices.reshape(16, 2, mesh.shape["tp"]), ("ep_0", "ep_1", "tp"))
    return jax.shard_map(
        shards,
        mesh=torus,
        in_specs=(
            P(EP, "tp"),
            P(EP, "tp"),
            P(EP, "tp"),
            P(),
            P(),
            P(),
            P(None, "tp"),
            P(EP, "tp"),
            P(),
            P(EP, None),
            P(EP, None),
            P(EP, None, "tp"),
            P(EP, None, "tp"),
            P(EP, None, "tp"),
        ),
        out_specs=(P(EP, "tp"), P(EP, "tp")),
        check_vma=False,
    )
```

profile of v0, /device:TPU:1, one launch (start us, length us, event | category | flops | bytes accessed | tf_op | source)
XLA Modules:
  0.0 310.1 jit_solution(1185379400146651329)
XLA Ops:
  9.4 1.4 pad_maximum_fusion.1
  15.4 2.4 scatter_custom_fusion
  17.9 2.8 gather_fusion
  20.9 10.5 %all_to_all.15 = bf16[16,2,1,22,256]{4,0,3,2,1:T(8,128)(2,1)S(1)} all-to-all(bf16[16,2,1,22,256]{4,0,3,2,1:T(8,128)(2,1)S(1)} %copy.45), channel_id=1, replica_groups=mesh['ep_0'=16,'ep_1'=2,'tp'=16] {'ep_1'}, dimensions={1} | all-to-all | bytes 720896 | tf_op jit(solution)/shard_map/all_to_all | solution.py:39
  32.5 9.6 %all-to-all-start.1 = ((bf16[16,2,1,22,256]{4,1,3,2,0:T(2,128)(2,1)}), bf16[16,2,1,22,256]{4,1,3,2,0:T(2,128)(2,1)S(1)}, u32[]{:S(2)}, u32[]{:S(2)}) async-start(bf16[16,2,1,22,256]{4,1,3,2,0:T(2,128)(2,1)} %copy.46), calls=%async_computation.1 | async-start | bytes 720896 | tf_op jit(solution)/shard_map/all_to_all | solution.py:39
  43.2 20.0 %all-to-all-done.1 = bf16[16,2,1,22,256]{4,1,3,2,0:T(2,128)(2,1)S(1)} async-done(((bf16[16,2,1,22,256]{4,1,3,2,0:T(2,128)(2,1)}), bf16[16,2,1,22,256]{4,1,3,2,0:T(2,128)(2,1)S(1)}, u32[]{:S(2)}, u32[]{:S(2)}) %all-to-all-start.1) | async-done | bytes 360480 | tf_op jit(solution)/shard_map/all_to_all | solution.py:39
  64.3 35.3 %all-gather.4.cloned.1.call-done = bf16[8192,128]{0,1:T(8,128)(2,1)} async-done(((bf16[256,128]{0,1:T(8,128)(2,1)}), bf16[8192,128]{0,1:T(8,128)(2,1)}) %all-gather.4.cloned.1.call-update) | async-done | bytes 2097168 | tf_op jit(solution)/shard_map/all_gather | solution.py:20
  99.5 1.7 fusion.70
  101.8 1.6 copy.39
  104.0 1.5 copy.40
  105.5 25.7 %while.15 = (s32[]{:T(128)}, f32[1,2,256]{2,1,0:T(2,128)S(1)}, f32[1,2,256]{2,1,0:T(2,128)S(1)}, f32[256,1,2,64]{0,3,2,1:T(8,128)S(1)}, bf16[8,1024,1,64]{1,3,2,...) while((s32[]{:T(128)}, f32[1,2,256]{2,1,0:T(2,128)S(1)}, ...), condition=%wide.region_5.6_spmd.clone, body=%wide.region_2.5_spmd.clone.sunk | while | flops 138513408 | bytes 6914169 | solution.py:135
  107.3 1.4 fusion.82
  110.5 1.4 fusion.82
  111.9 1.4 bitcast_reduce_fusion.3
  113.7 1.4 fusion.82
  117.0 1.4 fusion.82
  120.2 1.4 fusion.82
  123.4 1.4 fusion.82
  124.8 1.4 bitcast_reduce_fusion.3
  126.6 1.4 fusion.82
  129.8 1.4 fusion.82
  131.4 42.5 %all-gather.6.cloned.1.call-done = bf16[704,4096]{1,0:T(8,128)(2,1)} async-done(((bf16[704,256]{1,0:T(8,128)(2,1)}), bf16[704,4096]{1,0:T(8,128)(2,1)}) %all-gather.6.cloned.1.call-update) | async-done | bytes 5767184 | tf_op jit(solution)/shard_map/all_gather | solution.py:163
  173.9 4.0 %fusion.19 = f32[704]{0:T(1024)S(1)} fusion(bf16[704,4096]{1,0:T(8,128)(2,1)} %all-gather.6.cloned.1.call-done), kind=kLoop, calls=%fused_computation.32 | loop fusion | flops 8650048 | bytes 5769984 | tf_op jit(solution)/shard_map/reduce_sum | solution.py:170
  178.2 3.0 fusion.31
  181.2 1.7 fusion.40
  183.7 70.5 %all-gather.8.cloned.1.call-done = bf16[960,2048]{1,0:T(8,128)(2,1)} async-done(((bf16[960,128]{1,0:T(8,128)(2,1)}), bf16[960,2048]{1,0:T(8,128)(2,1)}) %all-gather.8.cloned.1.call-update) | async-done | bytes 3932176 | tf_op jit(solution)/shard_map/all_gather | solution.py:20
  254.2 2.7 fusion.28
  257.8 14.4 %all-to-all-start.2 = ((bf16[32,22,256]{2,1,0:T(8,128)(2,1)}), bf16[32,22,256]{2,1,0:T(8,128)(2,1)S(1)}, u32[]{:S(2)}, u32[]{:S(2)}) async-start(bf16[32,22,256]{2,1,0:T(8,128)(2,1)} %reshape.435), calls=%async_computation.2 | async-start | bytes 786432 | tf_op jit(solution)/shard_map/all_to_all | solution.py:188
  272.3 1.5 fusion.27
  273.8 2.3 fusion.43
  276.2 23.7 %all-to-all-done.2 = bf16[32,22,256]{2,1,0:T(8,128)(2,1)S(1)} async-done(((bf16[32,22,256]{2,1,0:T(8,128)(2,1)}), bf16[32,22,256]{2,1,0:T(8,128)(2,1)S(1)}, u32[]{:S(2)}, u32[]{:S(2)}) %all-to-all-start.2) | async-done | bytes 360480 | tf_op jit(solution)/shard_map/all_to_all | solution.py:188
  300.0 2.0 gather_fusion.1
  (122 shorter events, 26.7 us)
Async XLA Ops:
  7.2 247.0 %copy-start = (bf16[1,2048,256]{2,1,0:T(8,128)(2,1)S(1)}, bf16[1,2048,256]{2,1,0:T(8,128)(2,1)}, u32[]{:S(2)}) copy-start(bf16[1,2048,256]{2,1,0:T(8,128)(2,1)} %param.29) | copy-start | bytes 3145732
  7.2 92.3 %all-gather.4.cloned.1.call-start = ((), (), s32[]{:S(2)}) async-start(), calls=%async_computation.3 | async-start | bytes 2162688 | tf_op jit(solution)/shard_map/all_gather | solution.py:20
  17.9 24.3 %copy-start.2 = (bf16[256,128]{1,0:T(8,128)(2,1)S(1)}, bf16[256,128]{1,0:T(8,128)(2,1)}, u32[]{:S(2)}) copy-start(bf16[256,128]{1,0:T(8,128)(2,1)} %param.16) | copy-start | bytes 196612
  17.9 24.5 %copy-start.4 = (f32[64]{0:T(128)S(1)}, f32[64]{0:T(128)}, u32[]{:S(2)}) copy-start(f32[64]{0:T(128)} %param.19) | copy-start | bytes 772
  32.5 30.6 %all-to-all-start.1 = ((bf16[16,2,1,22,256]{4,1,3,2,0:T(2,128)(2,1)}), bf16[16,2,1,22,256]{4,1,3,2,0:T(2,128)(2,1)S(1)}, u32[]{:S(2)}, u32[]{:S(2)}) async-start(bf16[16,2,1,22,256]{4,1,3,2,0:T(2,128)(2,1)} %copy.46), calls=%async_computation.1 | async-start | bytes 720896 | tf_op jit(solution)/shard_map/all_to_all | solution.py:39
  42.1 131.8 %all-gather.6.cloned.1.call-start = ((), (), s32[]{:S(2)}) async-start(), calls=%async_computation.4 | async-start | bytes 6127616 | tf_op jit(solution)/shard_map/all_gather | solution.py:163
  64.0 190.1 %all-gather.8.cloned.1.call-start = ((), (), s32[]{:S(2)}) async-start(), calls=%async_computation.5 | async-start | bytes 4177920 | tf_op jit(solution)/shard_map/all_gather | solution.py:20
  131.2 46.7 %copy-start.7 = (f32[4096]{0:T(1024)S(1)}, f32[4096]{0:T(1024)}, u32[]{:S(2)}) copy-start(f32[4096]{0:T(1024)} %param.24) | copy-start | bytes 49156
  173.9 4.3 %copy-start.1 = (bf16[704,4096]{1,0:T(8,128)(2,1)S(1)}, bf16[704,4096]{1,0:T(8,128)(2,1)}, u32[]{:S(2)}) copy-start(bf16[704,4096]{1,0:T(8,128)(2,1)} %all-gather.6.cloned.1.call-done) | copy-start | bytes 17301508
  178.2 3.0 copy-start.5
  183.7 88.5 %copy-start.3 = (f32[256,2]{0,1:T(2,128)S(1)}, f32[256,2]{0,1:T(2,128)}, u32[]{:S(2)}) copy-start(f32[256,2]{0,1:T(2,128)} %param.26) | copy-start | bytes 6148
  183.7 90.1 %copy-start.6 = (bf16[2048,256]{1,0:T(8,128)(2,1)S(1)}, bf16[2048,256]{1,0:T(8,128)(2,1)}, u32[]{:S(2)}) copy-start(bf16[2048,256]{1,0:T(8,128)(2,1)} %param.22) | copy-start | bytes 3145732
  183.7 90.1 %copy-start.8 = (f32[2048]{0:T(1024)S(1)}, f32[2048]{0:T(1024)}, u32[]{:S(2)}) copy-start(f32[2048]{0:T(1024)} %param.21) | copy-start | bytes 24580
  257.8 42.1 %all-to-all-start.2 = ((bf16[32,22,256]{2,1,0:T(8,128)(2,1)}), bf16[32,22,256]{2,1,0:T(8,128)(2,1)S(1)}, u32[]{:S(2)}, u32[]{:S(2)}) async-start(bf16[32,22,256]{2,1,0:T(8,128)(2,1)} %reshape.435), calls=%async_computation.2 | async-start | bytes 786432 | tf_op jit(solution)/shard_map/all_to_all | solution.py:188
Sparse Core Ops, SparseCore 0:
  10.9 88.5 all-gather.3
  102.5 71.3 all-gather.5
  183.8 70.3 all-gather.7
where the time goes:
time: 311 us; the launch traced here: 310 us
  waiting for transfers between devices  192 us (62%)
  matrix products  31.9 us (10%)
  starting transfers between devices  24.3 us (8%)
  local copies, waits for them, and re-layouts  20.2 us (6%)
  other arithmetic  16.7 us (5%)
  between operations  14.2 us (5%)
  blocking collectives  10.5 us (3%)
    all_gather x2, waiting for transfers between devices, in_one_piece(): filled = lax.all_gather(both, axis, axis=dim, tiled=True)  106 us
    all_gather x1, waiting for transfers between devices, shards(): lax.all_gather(arrived, 'tp', axis=1, tiled=True).astype(jnp.float32)  42.5 us
    all_to_all x1, waiting for transfers between devices, shards(): lax.all_to_all(expert_back, EP, split_axis=0, concat_axis=0, tiled=True)  23.7 us
    all_to_all x1, waiting for transfers between devices, exchange_in_order(): filled = lax.all_to_all(filled, axes[k], k, k, tiled=True)  20 us
    all_to_all x1, starting transfers between devices, shards(): lax.all_to_all(expert_back, EP, split_axis=0, concat_axis=0, tiled=True)  14.4 us
    dot_general x8, matrix products, absorb(): jnp.einsum('hgrn,nhd->rhgd', rounded, value_block, preferred_element_type...  11.1 us
    dot_general x8, matrix products, absorb(): jnp.einsum('rhgd,nhd->hgrn', query_heads, key_block, preferred_element_ty...  11 us
    all_to_all x1, blocking collectives, exchange_in_order(): filled = lax.all_to_all(filled, axes[k], k, k, tiled=True)  10.5 us
  transfers between devices with their start and end apart: 5, of which 5 were waited for; matrix products, arithmetic and copies ran while one was open for 16% of the time, Pallas kernels for 0%

commit v1 on v0

--- a/solution.py
+++ b/solution.py
@@ -160,7 +160,13 @@
     arrived = exchange_by_chip(outgoing, ("ep_0", "ep_1"), (1, 0), 0, 0).reshape(
         slot_total, width_local
     )
-    piece_float = lax.all_gather(arrived, "tp", axis=1, tiled=True).astype(jnp.float32)
+
+    def compute_the_rates(target):
+        s_next = tuple((target for _ in range(jax.lax.axis_size("tp"))))
+        h_now = jnp.concatenate(s_next, 1)
+        return jax.lax.all_to_all(h_now, split_axis=1, axis_name="tp", concat_axis=1, tiled=True)
+
+    piece_float = compute_the_rates(arrived).astype(jnp.float32)
     gain_piece = expert_gain
     scaled_piece = (piece_float * gain_piece).astype(jnp.bfloat16)
     gate_rows = expert_gate[0]

time: 311 us -> 295 us (0.949)
  waiting for transfers between devices: 192 us -> 166 us
  starting transfers between devices: 24.3 us -> 29.6 us
  local copies, waits for them, and re-layouts: 20.2 us -> 23.6 us
    all_gather x1 -> x0, waiting for transfers between devices: 42.5 us -> none  [shards(): lax.all_gather(arrived, 'tp', axis=1, tiled=True).astype(jnp.float32)]
    all_to_all x0 -> x1, waiting for transfers between devices: none -> 9.39 us  [compute_the_rates(): jax.lax.all_to_all(h_now, split_axis=1, axis_name='tp', concat_axis=1, ti...]
    all_gather x2, waiting for transfers between devices: 106 us -> 113 us  [in_one_piece(): filled = lax.all_gather(both, axis, axis=dim, tiled=True)]
    all_to_all x0 -> x1, starting transfers between devices: none -> 5.37 us  [compute_the_rates(): jax.lax.all_to_all(h_now, split_axis=1, axis_name='tp', concat_axis=1, ti...]
    concatenate x0 -> x2, local copies, waits for them, and re-layouts: none -> 3.22 us  [compute_the_rates(): h_now = jnp.concatenate(s_next, 1)]
  transfers between devices with their start and end apart: 5 -> 5, of which waited for: 5 -> 5; matrix products, arithmetic and copies ran while one was open for 16% -> 17% of each run, Pallas kernels for 0% -> 0%
where the time goes in v1:
time: 295 us; the launch traced here: 294 us
  waiting for transfers between devices  166 us (56%)
  matrix products  30.5 us (10%)
  starting transfers between devices  29.6 us (10%)
  local copies, waits for them, and re-layouts  23.6 us (8%)
  other arithmetic  19.3 us (7%)
  between operations  14.5 us (5%)
  blocking collectives  10.5 us (4%)
    all_gather x2, waiting for transfers between devices, in_one_piece(): filled = lax.all_gather(both, axis, axis=dim, tiled=True)  113 us
    all_to_all x1, waiting for transfers between devices, shards(): lax.all_to_all(expert_back, EP, split_axis=0, concat_axis=0, tiled=True)  23.6 us
    all_to_all x1, waiting for transfers between devices, exchange_in_order(): filled = lax.all_to_all(filled, axes[k], k, k, tiled=True)  19.9 us
    all_to_all x1, starting transfers between devices, shards(): lax.all_to_all(expert_back, EP, split_axis=0, concat_axis=0, tiled=True)  14.4 us
    dot_general x8, matrix products, absorb(): jnp.einsum('hgrn,nhd->rhgd', rounded, value_block, preferred_element_type...  11.1 us
    dot_general x8, matrix products, absorb(): jnp.einsum('rhgd,nhd->hgrn', query_heads, key_block, preferred_element_ty...  11 us
    all_to_all x1, blocking collectives, exchange_in_order(): filled = lax.all_to_all(filled, axes[k], k, k, tiled=True)  10.5 us
    all_to_all x1, starting transfers between devices, exchange_in_order(): filled = lax.all_to_all(filled, axes[k], k, k, tiled=True)  9.57 us
  transfers between devices with their start and end apart: 5, of which 5 were waited for; matrix products, arithmetic and copies ran while one was open for 17% of the time, Pallas kernels for 0%

profile of v1, /device:TPU:1, one launch (start us, length us, event | category | flops | bytes accessed | tf_op | source)
XLA Modules:
  0.0 294.3 jit_solution(8911861369216282384)
XLA Ops:
  9.4 1.4 pad_maximum_fusion.1
  15.4 2.4 scatter_custom_fusion
  17.9 2.8 gather_fusion
  20.9 10.5 %all_to_all.21 = bf16[16,2,1,22,256]{4,0,3,2,1:T(8,128)(2,1)S(1)} all-to-all(bf16[16,2,1,22,256]{4,0,3,2,1:T(8,128)(2,1)S(1)} %copy.61), channel_id=1, replica_groups=mesh['ep_0'=16,'ep_1'=2,'tp'=16] {'ep_1'}, dimensions={1} | all-to-all | bytes 720896 | tf_op jit(solution)/shard_map/all_to_all | solution.py:39
  32.5 9.6 %all-to-all-start.1 = ((bf16[16,2,1,22,256]{4,1,3,2,0:T(2,128)(2,1)}), bf16[16,2,1,22,256]{4,1,3,2,0:T(2,128)(2,1)S(1)}, u32[]{:S(2)}, u32[]{:S(2)}) async-start(bf16[16,2,1,22,256]{4,1,3,2,0:T(2,128)(2,1)} %copy.62), calls=%async_computation.1 | async-start | bytes 720896 | tf_op jit(solution)/shard_map/all_to_all | solution.py:39
  43.1 19.9 %all-to-all-done.1 = bf16[16,2,1,22,256]{4,1,3,2,0:T(2,128)(2,1)S(1)} async-done(((bf16[16,2,1,22,256]{4,1,3,2,0:T(2,128)(2,1)}), bf16[16,2,1,22,256]{4,1,3,2,0:T(2,128)(2,1)S(1)}, u32[]{:S(2)}, u32[]{:S(2)}) %all-to-all-start.1) | async-done | bytes 360480 | tf_op jit(solution)/shard_map/all_to_all | solution.py:39
  63.2 3.1 %concatenate.55 = bf16[704,16,256]{2,0,1:T(8,128)(2,1)} broadcast(bf16[704,256]{1,0:T(8,128)(2,1)S(1)} %concatenate.54), dimensions={0,2} | broadcast | bytes 6127616 | tf_op jit(solution)/shard_map/concatenate | solution.py:166
  66.3 5.4 %all-to-all-start.2 = ((bf16[704,16,256]{2,0,1:T(8,128)(2,1)}), bf16[704,16,256]{2,0,1:T(8,128)(2,1)}, u32[]{:S(2)}, u32[]{:S(2)}) async-start(bf16[704,16,256]{2,0,1:T(8,128)(2,1)} %concatenate.55), calls=%async_computation.2 | async-start | bytes 11534336 | tf_op jit(solution)/shard_map/all_to_all | solution.py:167
  71.9 27.6 %all-gather.3.cloned.1.call-done = bf16[8192,128]{0,1:T(8,128)(2,1)} async-done(((bf16[256,128]{0,1:T(8,128)(2,1)}), bf16[8192,128]{0,1:T(8,128)(2,1)}) %all-gather.3.cloned.1.call-update) | async-done | bytes 2097168 | tf_op jit(solution)/shard_map/all_gather | solution.py:20
  99.5 1.7 fusion.57
  101.8 1.5 copy.55
  104.0 1.6 copy.56
  105.6 25.6 %while.15 = (s32[]{:T(128)}, f32[1,2,256]{2,1,0:T(2,128)S(1)}, f32[1,2,256]{2,1,0:T(2,128)S(1)}, f32[256,1,2,64]{0,3,2,1:T(8,128)S(1)}, bf16[8,1024,1,64]{1,3,2,...) while((s32[]{:T(128)}, f32[1,2,256]{2,1,0:T(2,128)S(1)}, ...), condition=%wide.region_5.6_spmd.clone, body=%wide.region_2.5_spmd.clone.sunk | while | flops 138513408 | bytes 6914169 | solution.py:135
  107.4 1.4 fusion.71
  110.6 1.4 fusion.71
  113.8 1.4 fusion.71
  117.0 1.4 fusion.71
  120.2 1.4 fusion.71
  123.4 1.4 fusion.71
  126.6 1.4 fusion.71
  129.8 1.4 fusion.71
  131.4 9.4 %all-to-all-done.2 = bf16[704,16,256]{2,0,1:T(8,128)(2,1)} async-done(((bf16[704,16,256]{2,0,1:T(8,128)(2,1)}), bf16[704,16,256]{2,0,1:T(8,128)(2,1)}, u32[]{:S(2)}, u32[]{:S(2)}) %all-to-all-start.2) | async-done | bytes 5767200 | tf_op jit(solution)/shard_map/all_to_all | solution.py:167
  140.8 6.5 %fusion.19 = (f32[704]{0:T(1024)S(1)}, bf16[16,88,8,256]{3,2,1,0:T(8,128)(2,1)S(1)}) fusion(bf16[704,16,256]{2,0,1:T(8,128)(2,1)} %all-to-all-done.2, f32[16,256]{1,0:T(8,128)S(1)} %mul.300), kind=kLoop, calls=%fused_computation.32 | loop fusion | flops 14417216 | bytes 11553536 | tf_op jit(solution)/shard_map/reduce_sum | solution.py:176
  148.5 1.7 convolution_multiply_fusion.1
  150.2 1.7 fusion.29
  152.7 85.4 %all-gather.5.cloned.1.call-done = bf16[960,2048]{1,0:T(8,128)(2,1)} async-done(((bf16[960,128]{1,0:T(8,128)(2,1)}), bf16[960,2048]{1,0:T(8,128)(2,1)}) %all-gather.5.cloned.1.call-update) | async-done | bytes 3932176 | tf_op jit(solution)/shard_map/all_gather | solution.py:20
  238.1 2.7 fusion.25
  241.7 14.4 %all-to-all-start.3 = ((bf16[32,22,256]{2,1,0:T(8,128)(2,1)}), bf16[32,22,256]{2,1,0:T(8,128)(2,1)S(1)}, u32[]{:S(2)}, u32[]{:S(2)}) async-start(bf16[32,22,256]{2,1,0:T(8,128)(2,1)} %reshape.482), calls=%async_computation.3 | async-start | bytes 786432 | tf_op jit(solution)/shard_map/all_to_all | solution.py:194
  256.2 1.5 fusion.24
  257.8 2.3 fusion.30
  260.1 23.6 %all-to-all-done.3 = bf16[32,22,256]{2,1,0:T(8,128)(2,1)S(1)} async-done(((bf16[32,22,256]{2,1,0:T(8,128)(2,1)}), bf16[32,22,256]{2,1,0:T(8,128)(2,1)S(1)}, u32[]{:S(2)}, u32[]{:S(2)}) %all-to-all-start.3) | async-done | bytes 360480 | tf_op jit(solution)/shard_map/all_to_all | solution.py:194
  283.9 2.0 gather_fusion.1
  (124 shorter events, 29.5 us)
Async XLA Ops:
  7.2 230.9 %copy-start = (bf16[1,2048,256]{2,1,0:T(8,128)(2,1)S(1)}, bf16[1,2048,256]{2,1,0:T(8,128)(2,1)}, u32[]{:S(2)}) copy-start(bf16[1,2048,256]{2,1,0:T(8,128)(2,1)} %param.29) | copy-start | bytes 3145732
  7.2 92.3 %all-gather.3.cloned.1.call-start = ((), (), s32[]{:S(2)}) async-start(), calls=%async_computation.4 | async-start | bytes 2162688 | tf_op jit(solution)/shard_map/all_gather | solution.py:20
  17.9 24.3 %copy-start.2 = (f32[4096]{0:T(1024)S(1)}, f32[4096]{0:T(1024)}, u32[]{:S(2)}) copy-start(f32[4096]{0:T(1024)} %param.24) | copy-start | bytes 49156
  17.9 24.3 %copy-start.1 = (bf16[256,128]{1,0:T(8,128)(2,1)S(1)}, bf16[256,128]{1,0:T(8,128)(2,1)}, u32[]{:S(2)}) copy-start(bf16[256,128]{1,0:T(8,128)(2,1)} %param.16) | copy-start | bytes 196612
  17.9 24.5 %copy-start.4 = (f32[64]{0:T(128)S(1)}, f32[64]{0:T(128)}, u32[]{:S(2)}) copy-start(f32[64]{0:T(128)} %param.19) | copy-start | bytes 772
  32.5 30.5 %all-to-all-start.1 = ((bf16[16,2,1,22,256]{4,1,3,2,0:T(2,128)(2,1)}), bf16[16,2,1,22,256]{4,1,3,2,0:T(2,128)(2,1)S(1)}, u32[]{:S(2)}, u32[]{:S(2)}) async-start(bf16[16,2,1,22,256]{4,1,3,2,0:T(2,128)(2,1)} %copy.62), calls=%async_computation.1 | async-start | bytes 720896 | tf_op jit(solution)/shard_map/all_to_all | solution.py:39
  66.3 74.5 %all-to-all-start.2 = ((bf16[704,16,256]{2,0,1:T(8,128)(2,1)}), bf16[704,16,256]{2,0,1:T(8,128)(2,1)}, u32[]{:S(2)}, u32[]{:S(2)}) async-start(bf16[704,16,256]{2,0,1:T(8,128)(2,1)} %concatenate.55), calls=%async_computation.2 | async-start | bytes 11534336 | tf_op jit(solution)/shard_map/all_to_all | solution.py:167
  71.7 166.4 %all-gather.5.cloned.1.call-start = ((), (), s32[]{:S(2)}) async-start(), calls=%async_computation.5 | async-start | bytes 4177920 | tf_op jit(solution)/shard_map/all_gather | solution.py:20
  147.3 1.2 copy-start.5
  148.5 1.7 copy-start.6
  152.6 103.4 %copy-start.3 = (f32[256,2]{0,1:T(2,128)S(1)}, f32[256,2]{0,1:T(2,128)}, u32[]{:S(2)}) copy-start(f32[256,2]{0,1:T(2,128)} %param.26) | copy-start | bytes 6148
  152.6 105.1 %copy-start.7 = (bf16[2048,256]{1,0:T(8,128)(2,1)S(1)}, bf16[2048,256]{1,0:T(8,128)(2,1)}, u32[]{:S(2)}) copy-start(bf16[2048,256]{1,0:T(8,128)(2,1)} %param.22) | copy-start | bytes 3145732
  152.6 105.1 %copy-start.8 = (f32[2048]{0:T(1024)S(1)}, f32[2048]{0:T(1024)}, u32[]{:S(2)}) copy-start(f32[2048]{0:T(1024)} %param.21) | copy-start | bytes 24580
  241.7 42.1 %all-to-all-start.3 = ((bf16[32,22,256]{2,1,0:T(8,128)(2,1)}), bf16[32,22,256]{2,1,0:T(8,128)(2,1)S(1)}, u32[]{:S(2)}, u32[]{:S(2)}) async-start(bf16[32,22,256]{2,1,0:T(8,128)(2,1)} %reshape.482), calls=%async_computation.3 | async-start | bytes 786432 | tf_op jit(solution)/shard_map/all_to_all | solution.py:194
Sparse Core Ops, SparseCore 0:
  10.9 88.5 all-gather.2
  152.7 85.3 all-gather.4
